TPU v7x, 32 devices: a whole 2x2x4 slice. The times are simulated.
32 devices in a mesh: sp: 16 (over z, y, x), tp: 2 (over core).
Axes of the slice: x: 2, y: 2, z: 4, core: 2. Of those that a mesh axis runs over, the one named last changes fastest.
Arguments:
- stream: bfloat16 [4096, 2048], P(('sp', 'tp')), may hold values from -6 to 6
- outer_gate: bfloat16 [4096, 1024], P('sp', 'tp'), may hold values from -6 to 6
- inner_gate: bfloat16 [4096, 1024], P('sp', 'tp'), may hold values from -6 to 6
- conv_values: bfloat16 [4096, 1024], P('sp', 'tp'), may hold values from -6 to 6
- doc_ids: int32 [4096], P('sp'), may hold values from 0 to 7, never falling along the last dimension, each value on 1 to 1024 neighbouring positions
- conv_taps: float32 [3, 1024], P(None, 'tp'), may hold values from -3.5 to 3.5
- out_weight: bfloat16 [1024, 2048], replicated, may hold values from -0.1875 to 0.1875
- norm_gain: float32 [2048], replicated, may hold values from 0.1 to 1.9
- route_ids: int32 [4096, 2], P(('sp', 'tp')), may hold values from 0 to 31, all different within a row; in each aligned block of 128 rows (0 to 127, 128 to 255, ...) at most 16 rows name the same one
- route_logits: float32 [4096, 2], P(('sp', 'tp')), may hold values from -4 to 4
- group_weight: float32 [4096], P(('sp', 'tp')), may hold values from 0.25 to 1
- w_gate: bfloat16 [32, 2048, 1024], P(('sp', 'tp')), may hold values from -0.125 to 0.125
- w_up: bfloat16 [32, 2048, 1024], P(('sp', 'tp')), may hold values from -0.125 to 0.125
- w_down: bfloat16 [32, 1024, 2048], P(('sp', 'tp')), may hold values from -0.1875 to 0.1875
Outputs:
- result: bfloat16 [4096, 2048], P(('sp', 'tp'))
Inputs may be any that keep to these rules, and one draw needn't show every extreme that they name: `route_ids`: the two experts of a token differ. In the rows of one device (aligned blocks of 128 rows) no expert is named more than 16 times, a bound that some block reaches. `doc_ids`: document numbers never fall along the sequence; a document has 1 to 1024 positions and one has exactly 1024.
All inputs are finite; a program needn't handle non-finite values.
Results may differ from a plain program's by a relative error of at most 0.0052.
Values may be sent and summed in bfloat16 or wider, within the bound.
No kernel may reach another device: no remote copies, remote signals or barrier semaphores. Data moves between devices by JAX's collectives and lax.ppermute only.
A program may use at most 64 MiB of HBM per device.

v0:
```python
import jax
import jax.numpy as jnp
from jax import lax
from jax.sharding import PartitionSpec as P


def padded_2(shard, sides, width):
    for axis, dim in sides:
        size, length = (lax.axis_size(axis), shard.shape[dim])
        up = [(i, (i + 1) % size) for i in range(size - 1)]
        down = [(j, i) for i, j in up]
        last = lax.slice_in_dim(shard, length - width, length, axis=dim)
        leading = lax.slice_in_dim(shard, 0, width, axis=dim)
        before = lax.ppermute(last, axis, up)
        after = lax.ppermute(leading, axis, down)
        shard = jnp.concatenate([before, shard, after], axis=dim)
    return shard


def on_device(
    stream,
    outer_gate,
    inner_gate,
    conv_values,
    doc_ids,
    conv_taps,
    out_weight,
    norm_gain,
    route_ids,
    route_logits,
    group_weight,
    w_gate,
    w_up,
    w_down,
):
    tok_rows = stream.shape[0]
    width = stream.shape[1]
    product = (inner_gate.astype(jnp.float32) * conv_values.astype(jnp.float32)).astype(
        jnp.bfloat16
    )
    doc_float = doc_ids.astype(jnp.bfloat16)
    padded, padded_docs = (padded_2(product, (("sp", 0),), 1), padded_2(doc_float, (("sp", 0),), 1))
    same_prev = (padded_docs[:-2] == doc_float).astype(jnp.float32)[:, None]
    same_next = (padded_docs[2:] == doc_float).astype(jnp.float32)[:, None]
    conv = (
        conv_taps[0] * padded[:-2].astype(jnp.float32) * same_prev
        + conv_taps[1] * product.astype(jnp.float32)
        + conv_taps[2] * padded[2:].astype(jnp.float32) * same_next
    )
    mixed = (outer_gate.astype(jnp.float32) * conv).astype(jnp.bfloat16)
    channels = lax.all_to_all(mixed, "tp", split_axis=0, concat_axis=1, tiled=True)
    projected = jnp.dot(channels, out_weight, preferred_element_type=jnp.float32)
    resid = stream.astype(jnp.float32) + projected
    scale = lax.rsqrt(jnp.mean(resid * resid, axis=-1, keepdims=True) + 1e-06)
    normed = (resid * scale * norm_gain).astype(jnp.bfloat16)
    expert_total = lax.axis_size("sp") * lax.axis_size("tp")
    top_count = route_ids.shape[1]
    capacity = 2 * tok_rows * top_count // expert_total
    flat_ids = route_ids.reshape(-1)
    one_hot = (flat_ids[:, None] == jnp.arange(expert_total, dtype=jnp.int32)[None, :]).astype(
        jnp.int32
    )
    rank = jnp.sum((jnp.cumsum(one_hot, axis=0) - 1) * one_hot, axis=1)
    slot = flat_ids * capacity + rank
    slot_count = expert_total * capacity
    source_row = (
        jnp.zeros((slot_count,), jnp.int32)
        .at[slot]
        .set(jnp.arange(flat_ids.shape[0], dtype=jnp.int32) // top_count)
    )
    filled = jnp.zeros((slot_count,), jnp.bool_).at[slot].set(True)
    outgoing = jnp.where(filled[:, None], normed[source_row], jnp.zeros((), jnp.bfloat16)).reshape(
        expert_total, capacity, width
    )
    arrived = lax.all_to_all(outgoing, ("sp", "tp"), split_axis=0, concat_axis=0, tiled=True)
    sources, items, features = arrived.shape
    rows_in = arrived.reshape(sources * items, features)
    hidden = (
        jax.nn.silu(jnp.dot(rows_in, w_gate[0], preferred_element_type=jnp.float32))
        * jnp.dot(rows_in, w_up[0], preferred_element_type=jnp.float32)
    ).astype(jnp.bfloat16)
    outputs = jnp.dot(hidden, w_down[0], preferred_element_type=jnp.float32).astype(jnp.bfloat16)
    returned = lax.all_to_all(
        outputs.reshape(sources, items, features),
        ("sp", "tp"),
        split_axis=0,
        concat_axis=0,
        tiled=True,
    )
    picked = (
        returned.reshape(slot_count, width)[slot]
        .astype(jnp.float32)
        .reshape(tok_rows, top_count, width)
    )
    expo = jnp.exp(route_logits)
    gate = group_weight[:, None] * expo / jnp.sum(expo, axis=1, keepdims=True)
    result = resid + jnp.sum(gate[:, :, None] * picked, axis=1)
    return result.astype(jnp.bfloat16)


def solution(mesh):
    placed = (
        P(("sp", "tp"), None),
        P("sp", "tp"),
        P("sp", "tp"),
        P("sp", "tp"),
        P("sp"),
        P(None, "tp"),
        P(),
        P(),
        P(("sp", "tp"), None),
        P(("sp", "tp"), None),
        P(("sp", "tp")),
        P(("sp", "tp"), None, None),
        P(("sp", "tp"), None, None),
        P(("sp", "tp"), None, None),
    )
    return jax.shard_map(
        on_device, mesh=mesh, in_specs=placed, out_specs=P(("sp", "tp"), None), check_vma=False
    )
```

profile of v0, /device:TPU:0, one launch (start us, length us, event | category | flops | bytes accessed | tf_op | source)
XLA Modules:
  0.0 169.3 jit_solution(4151391438809360174)
XLA Ops:
  0.0 0.7 convert_element_type.66
  0.7 0.6 fusion.23
  1.3 5.4 %collective-permute-start.1 = (bf16[1]{0:T(256)(128)(2,1)}, bf16[1]{0:T(256)(128)(2,1)}, u32[]{:S(2)}, u32[]{:S(2)}) collective-permute-start(bf16[1]{0:T(256)(128)(2,1)} %get-tuple-element.14), channel_id=1, source_target_pairs={{0,2},{2,4},{4,6},{6,8},{8,10},{10,12},{12,14},{14,16},{16,18},{18... | collective-permute-start | bytes 14 | tf_op jit(solution)/shard_map/ppermute | solution.py:14
  6.7 1.3 collective-permute-start.3
  8.0 1.1 multiply_convert_fusion.3
  9.1 4.5 %collective-permute-start = (bf16[1,512]{1,0:T(2,128)(2,1)S(1)}, bf16[1,512]{1,0:T(2,128)(2,1)S(1)}, u32[]{:S(2)}, u32[]{:S(2)}) collective-permute-start(bf16[1,512]{1,0:T(2,128)(2,1)S(1)} %get-tuple-element.5), channel_id=1, source_target_pairs={{0,2},{2,4},{4,6},{6,8},{8,10},{10,12},{12,14},{14,16},{16,18},{18... | collective-permute-start | bytes 3080 | tf_op jit(solution)/shard_map/ppermute | solution.py:14
  13.7 1.3 collective-permute-start.2
  15.0 0.8 copy.24
  15.8 0.1 eq.37
  15.9 0.1 eq.33
  16.0 0.7 broadcast_multiply_fusion
  16.7 0.8 fusion.22
  17.5 0.6 reduce-window.6
  18.1 0.2 slice_reduce_fusion
  18.4 0.1 copy.23
  18.5 0.1 mul.133
  18.6 0.1 fusion.14
  18.7 1.4 scatter_custom_fusion.1
  20.2 1.5 scatter_custom_fusion
  21.7 0.1 broadcast_in_dim.22
  21.8 0.0 collective-permute-done.1
  21.8 0.0 collective-permute-done.3
  21.8 1.3 pad_maximum_fusion.2
  23.0 0.8 compare_convert_fusion.1
  23.8 0.0 collective-permute-done
  23.8 0.0 collective-permute-done.2
  23.8 1.2 multiply_convert_fusion.2
  25.0 3.9 %all_to_all.29 = bf16[2,128,512]{2,1,0:T(8,128)(2,1)S(1)} all-to-all(bf16[2,128,512]{2,1,0:T(8,128)(2,1)S(1)} %bitcast.51), channel_id=1, replica_groups=mesh['sp'=16,'tp'=2] {'tp'}, dimensions={0} | all-to-all | bytes 524288 | tf_op jit(solution)/shard_map/all_to_all | solution.py:51
  29.0 0.2 copy.21
  29.1 0.0 copy-done
  29.2 0.0 copy-start.1
  29.2 3.0 %multiply_reduce_fusion.1 = (f32[128]{0:T(128)S(1)}, f32[128,2048]{1,0:T(8,128)S(1)}) fusion(bf16[128,1024]{0,1:T(8,128)(2,1)S(1)} %bitcast.52, bf16[1024,2048]{1,0:T(8,128)(2,1)} %param.20, bf16[128,2048]{1,0:T(8,128)(2,1)S(1)} %copy-done), kind=kOutput, calls=%fused_computation.17 | convolution fusion | flops 537919360 | bytes 6029824 | tf_op jit(solution)/shard_map/dot_general | solution.py:52
  32.2 0.0 copy-done.1
  32.2 0.2 multiply_convert_fusion.1
  32.4 3.3 %gather_fusion = bf16[512,2048]{1,0:T(8,128)(2,1)} fusion(bf16[128,2048]{1,0:T(8,128)(2,1)S(1)} %multiply_convert_fusion.1, s32[1024]{0:T(1024)S(1)} %pad_clamp_fusion.1), kind=kCustom, calls=%fused_computation | custom fusion | bytes 4196352 | tf_op jit(solution)/shard_map/gather | solution.py:72
  35.7 1.8 %broadcast_select_fusion = bf16[32,16,2048]{2,1,0:T(8,128)(2,1)S(1)} fusion(bf16[32,16,2048]{2,1,0:T(8,128)(2,1)} %bitcast.47, pred[32,16]{1,0:T(8,128)(4,1)S(1)} %broadcast_in_dim.22), kind=kLoop, calls=%fused_computation.14 | loop fusion | flops 1048576 | bytes 4194816 | tf_op jit(solution)/shard_map/jit(_where)/select_n | solution.py:72
  37.5 0.0 copy-start.4
  37.5 56.7 %all_to_all.30 = bf16[32,16,2048]{2,1,0:T(8,128)(2,1)S(1)} all-to-all(bf16[32,16,2048]{2,1,0:T(8,128)(2,1)S(1)} %broadcast_select_fusion), channel_id=1, replica_groups=mesh['sp'=16,'tp'=2] {'sp','tp'}, dimensions={0} | all-to-all | bytes 4194304 | tf_op jit(solution)/shard_map/all_to_all | solution.py:75
  94.3 0.0 copy-done.4
  94.3 3.7 %fusion.4 = f32[512,1024]{1,0:T(8,128)} fusion(bf16[512,2048]{1,0:T(8,128)(2,1)S(1)} %bitcast.49, bf16[1,2048,1024]{2,1,0:T(8,128)(2,1)S(1)} %copy-done.4), kind=kOutput, calls=%fused_computation.8 | convolution fusion | flops 2147483648 | bytes 8388608 | tf_op jit(solution)/shard_map/dot_general | solution.py:79
  98.0 9.9 %fusion.6 = bf16[512,2048]{1,0:T(8,128)(2,1)} fusion(bf16[1,1024,2048]{2,1,0:T(8,128)(2,1)} %param.27, f32[512,1024]{1,0:T(8,128)} %fusion.4, bf16[512,2048]{1,0:T(8,128)(2,1)S(1)} %bitcast.50, bf16[1,2048,1024]{2,1,0:T(8,128)(2,1)} %param.26), kind=kOutput, calls=%fused_computation.10 | convolution fusion | flops 4299161600 | bytes 14680064 | tf_op jit(solution)/shard_map/dot_general | solution.py:82
  107.9 3.8 %all-to-all-start.2 = ((bf16[32,16,2048]{2,1,0:T(8,128)(2,1)}), bf16[32,16,2048]{2,1,0:T(8,128)(2,1)S(1)}, u32[]{:S(2)}, u32[]{:S(2)}) async-start(bf16[32,16,2048]{2,1,0:T(8,128)(2,1)} %bitcast.48), calls=%async_computation.2 | async-start | bytes 4194304 | tf_op jit(solution)/shard_map/all_to_all | solution.py:83
  111.8 0.1 copy.22
  111.9 48.5 %all-to-all-done.2 = bf16[32,16,2048]{2,1,0:T(8,128)(2,1)S(1)} async-done(((bf16[32,16,2048]{2,1,0:T(8,128)(2,1)}), bf16[32,16,2048]{2,1,0:T(8,128)(2,1)S(1)}, u32[]{:S(2)}, u32[]{:S(2)}) %all-to-all-start.2) | async-done | bytes 2097184 | tf_op jit(solution)/shard_map/all_to_all | solution.py:83
  160.4 2.3 %gather_fusion.1 = bf16[256,2048]{1,0:T(8,128)(2,1)} fusion(bf16[512,2048]{1,0:T(8,128)(2,1)S(1)} %bitcast.46, s32[1024]{0:T(1024)S(1)} %pad_clamp_fusion), kind=kCustom, calls=%fused_computation.1 | custom fusion | bytes 2098176 | tf_op jit(solution)/shard_map/gather | solution.py:91
  162.8 2.4 %reshape.90 = f32[128,2,2048]{2,1,0:T(2,128)S(1)} reshape(bf16[256,2048]{1,0:T(8,128)(2,1)} %gather_fusion.1) | data formatting | bytes 3145728 | tf_op jit(solution)/shard_map/convert_element_type | solution.py:92
  165.1 3.2 %multiply_reduce_fusion = f32[128,2048]{1,0:T(8,128)S(1)} fusion(f32[128,2,2048]{2,1,0:T(2,128)S(1)} %reshape.90, f32[128,2]{1,0:T(8,128)S(1)} %copy.22), kind=kLoop, calls=%fused_computation.12 | loop fusion | flops 786432 | bytes 3146752 | tf_op jit(solution)/shard_map/reduce_sum | solution.py:97
  168.3 0.9 add_convert_fusion
  (18 shorter events, 0.1 us)
Async XLA Ops:
  0.0 29.2 %copy-start = (bf16[128,2048]{1,0:T(8,128)(2,1)S(1)}, bf16[128,2048]{1,0:T(8,128)(2,1)}, u32[]{:S(2)}) copy-start(bf16[128,2048]{1,0:T(8,128)(2,1)} %param.14) | copy-start | bytes 1572868
  1.3 20.4 %collective-permute-start.1 = (bf16[1]{0:T(256)(128)(2,1)}, bf16[1]{0:T(256)(128)(2,1)}, u32[]{:S(2)}, u32[]{:S(2)}) collective-permute-start(bf16[1]{0:T(256)(128)(2,1)} %get-tuple-element.14), channel_id=1, source_target_pairs={{0,2},{2,4},{4,6},{6,8},{8,10},{10,12},{12,14},{14,16},{16,18},{18... | collective-permute-start | bytes 14 | tf_op jit(solution)/shard_map/ppermute | solution.py:14
  6.7 15.1 %collective-permute-start.3 = (bf16[1]{0:T(256)(128)(2,1)}, bf16[1]{0:T(256)(128)(2,1)}, u32[]{:S(2)}, u32[]{:S(2)}) collective-permute-start(bf16[1]{0:T(256)(128)(2,1)} %get-tuple-element.15), channel_id=1, source_target_pairs={{2,0},{4,2},{6,4},{8,6},{10,8},{12,10},{14,12},{16,14},{18,16},{20... | collective-permute-start | bytes 14 | tf_op jit(solution)/shard_map/ppermute | solution.py:15
  9.1 14.7 %collective-permute-start = (bf16[1,512]{1,0:T(2,128)(2,1)S(1)}, bf16[1,512]{1,0:T(2,128)(2,1)S(1)}, u32[]{:S(2)}, u32[]{:S(2)}) collective-permute-start(bf16[1,512]{1,0:T(2,128)(2,1)S(1)} %get-tuple-element.5), channel_id=1, source_target_pairs={{0,2},{2,4},{4,6},{6,8},{8,10},{10,12},{12,14},{14,16},{16,18},{18... | collective-permute-start | bytes 3080 | tf_op jit(solution)/shard_map/ppermute | solution.py:14
  13.7 10.1 %collective-permute-start.2 = (bf16[1,512]{1,0:T(2,128)(2,1)S(1)}, bf16[1,512]{1,0:T(2,128)(2,1)S(1)}, u32[]{:S(2)}, u32[]{:S(2)}) collective-permute-start(bf16[1,512]{1,0:T(2,128)(2,1)S(1)} %get-tuple-element.6), channel_id=1, source_target_pairs={{2,0},{4,2},{6,4},{8,6},{10,8},{12,10},{14,12},{16,14},{18,16},{20... | collective-permute-start | bytes 3080 | tf_op jit(solution)/shard_map/ppermute | solution.py:15
  29.2 3.0 %copy-start.1 = (f32[2048]{0:T(1024)S(1)}, f32[2048]{0:T(1024)}, u32[]{:S(2)}) copy-start(f32[2048]{0:T(1024)} %param.21) | copy-start | bytes 24580
  37.5 56.7 %copy-start.4 = (bf16[1,2048,1024]{2,1,0:T(8,128)(2,1)S(1)}, bf16[1,2048,1024]{2,1,0:T(8,128)(2,1)}, u32[]{:S(2)}) copy-start(bf16[1,2048,1024]{2,1,0:T(8,128)(2,1)} %param.25) | copy-start | bytes 12582916
  107.9 3.8 %copy-start.2 = (f32[128,2]{0,1:T(2,128)S(1)}, f32[128,2]{0,1:T(2,128)}, u32[]{:S(2)}) copy-start(f32[128,2]{0,1:T(2,128)} %param.23) | copy-start | bytes 3076
  107.9 3.9 %copy-start.3 = (f32[128]{0:T(128)S(1)}, f32[128]{0:T(128)}, u32[]{:S(2)}) copy-start(f32[128]{0:T(128)} %param.24) | copy-start | bytes 1540
  107.9 52.5 %all-to-all-start.2 = ((bf16[32,16,2048]{2,1,0:T(8,128)(2,1)}), bf16[32,16,2048]{2,1,0:T(8,128)(2,1)S(1)}, u32[]{:S(2)}, u32[]{:S(2)}) async-start(bf16[32,16,2048]{2,1,0:T(8,128)(2,1)} %bitcast.48), calls=%async_computation.2 | async-start | bytes 4194304 | tf_op jit(solution)/shard_map/all_to_all | solution.py:83
where the time goes:
time: 170 us; the launch traced here: 169 us
  blocking collectives  60.7 us (36%)
  waiting for transfers between devices  48.5 us (29%)
  matrix products  16.6 us (10%)
  starting transfers between devices  16.3 us (10%)
  local copies, waits for them, and re-layouts  14.3 us (8%)
  other arithmetic  12.6 us (7%)
    all_to_all x1, blocking collectives, on_device(): lax.all_to_all(outgoing, ('sp', 'tp'), split_axis=0, concat_axis=0, tiled...  56.7 us
    all_to_all x1, waiting for transfers between devices, on_device(): lax.all_to_all(outputs.reshape(sources, items, features), ('sp', 'tp'), s...  48.5 us
    ppermute x2, starting transfers between devices, padded_2(): before = lax.ppermute(last, axis, up)  9.91 us
    dot_general x1, matrix products, on_device(): jnp.dot(hidden, w_down[0], preferred_element_type=jnp.float32)  9.9 us
    all_to_all x1, blocking collectives, on_device(): lax.all_to_all(mixed, 'tp', split_axis=0, concat_axis=1, tiled=True)  3.94 us
    all_to_all x1, starting transfers between devices, on_device(): lax.all_to_all(outputs.reshape(sources, items, features), ('sp', 'tp'), s...  3.83 us
    dot_general x1, matrix products, on_device(): jnp.dot(rows_in, w_gate[0], preferred_element_type=jnp.float32)  3.73 us
  transfers between devices with their start and end apart: 5, of which 1 were waited for; matrix products, arithmetic and copies ran while one was open for 6% of the time, Pallas kernels for 0%

commit v1 on v0

v1 whole, which is shorter than its diff:
```python
import jax
import jax.numpy as jnp
from jax import lax
from jax.sharding import PartitionSpec as P

CHUNKS = 1


def on_device(
    stream,
    outer_gate,
    inner_gate,
    conv_values,
    doc_ids,
    conv_taps,
    out_weight,
    norm_gain,
    route_ids,
    route_logits,
    group_weight,
    w_gate,
    w_up,
    w_down,
):
    f32, bf16 = jnp.float32, jnp.bfloat16
    tok_rows, width = stream.shape
    channels_here = inner_gate.shape[1]

    def gated(rows):
        return (inner_gate[rows].astype(f32) * conv_values[rows].astype(f32)).astype(bf16)

    sp = lax.axis_size("sp")
    up = [(i, (i + 1) % sp) for i in range(sp - 1)]
    down = [(j, i) for i, j in up]
    lanes = 128

    def edge(rows):
        doc = jnp.broadcast_to(doc_ids[rows].astype(bf16)[:, None], (1, lanes))
        return jnp.concatenate([gated(rows), doc], axis=1)

    before = lax.ppermute(edge(slice(-1, None)), "sp", up)
    after = lax.ppermute(edge(slice(0, 1)), "sp", down)

    expert_total = lax.axis_size("sp") * lax.axis_size("tp")
    top_count = route_ids.shape[1]
    capacity = 2 * tok_rows * top_count // expert_total
    slot_count = expert_total * capacity
    names = jnp.arange(expert_total, dtype=jnp.int32)
    hits = [route_ids[:, k][:, None] == names[None, :] for k in range(top_count)]
    named = sum(h.astype(bf16) for h in hits)
    row_at = lax.broadcasted_iota(jnp.int32, (tok_rows, tok_rows), 0)
    col_at = lax.broadcasted_iota(jnp.int32, (tok_rows, tok_rows), 1)
    earlier = jnp.dot((col_at < row_at).astype(bf16), named, preferred_element_type=f32)
    rank = jnp.stack([jnp.sum(jnp.where(h, earlier, 0.0), axis=1) for h in hits]).astype(jnp.int32)
    ids = jnp.stack([route_ids[:, k] for k in range(top_count)])
    part = capacity // CHUNKS
    slot = (rank // part) * (expert_total * part) + ids * part + rank % part
    expo = jnp.exp(route_logits)
    gate = group_weight[:, None] * expo / jnp.sum(expo, axis=1, keepdims=True)

    product = gated(slice(None))
    prod = product.astype(f32)
    doc_before = before[:, channels_here].astype(jnp.int32)
    doc_after = after[:, channels_here].astype(jnp.int32)
    docs_prev = jnp.concatenate([doc_before, doc_ids[:-1]])
    docs_next = jnp.concatenate([doc_ids[1:], doc_after])
    same_prev = (docs_prev == doc_ids).astype(f32)[:, None]
    same_next = (docs_next == doc_ids).astype(f32)[:, None]
    prod_prev = jnp.concatenate([before[:, :channels_here], product[:-1]], axis=0).astype(f32)
    prod_next = jnp.concatenate([product[1:], after[:, :channels_here]], axis=0).astype(f32)
    conv = (
        conv_taps[0] * prod_prev * same_prev
        + conv_taps[1] * prod
        + conv_taps[2] * prod_next * same_next
    )
    mixed = (outer_gate.astype(f32) * conv).astype(bf16)
    halves = lax.all_to_all(
        mixed.reshape(-1, tok_rows, channels_here), "tp", split_axis=0, concat_axis=0, tiled=True
    )
    weights = out_weight.reshape(-1, channels_here, width)
    resid = stream.astype(f32)
    for i in range(weights.shape[0]):
        resid = resid + jnp.dot(halves[i], weights[i], preferred_element_type=f32)
    scale = lax.rsqrt(jnp.mean(resid * resid, axis=-1, keepdims=True) + 1e-06)
    normed = (resid * scale * norm_gain).astype(bf16)

    chunk_slots = expert_total * part
    result = resid
    arrived = []
    for c in range(CHUNKS):
        at = c * chunk_slots + lax.broadcasted_iota(jnp.int32, (chunk_slots, tok_rows), 0)
        pick = sum((at == slot[k][None, :]).astype(bf16) for k in range(top_count))
        outgoing = jnp.dot(pick, normed, preferred_element_type=f32).astype(bf16)
        arrived.append(
            lax.all_to_all(
                outgoing.reshape(expert_total, part, width),
                ("sp", "tp"), split_axis=0, concat_axis=0, tiled=True,
            )
        )
    returned = []
    for c in range(CHUNKS):
        rows_in = arrived[c].reshape(chunk_slots, width)
        hidden = (
            jax.nn.silu(jnp.dot(rows_in, w_gate[0], preferred_element_type=f32))
            * jnp.dot(rows_in, w_up[0], preferred_element_type=f32)
        ).astype(bf16)
        outputs = jnp.dot(hidden, w_down[0], preferred_element_type=f32).astype(bf16)
        returned.append(
            lax.all_to_all(
                outputs.reshape(expert_total, part, width),
                ("sp", "tp"), split_axis=0, concat_axis=0, tiled=True,
            )
        )
    for c in range(CHUNKS):
        at = c * chunk_slots + lax.broadcasted_iota(jnp.int32, (tok_rows, chunk_slots), 1)
        spread = sum(
            jnp.where(at == slot[k][:, None], gate[:, k][:, None], 0.0) for k in range(top_count)
        )
        high = lax.reduce_precision(spread, 8, 7)
        both = jnp.concatenate([high.astype(bf16), (spread - high).astype(bf16)], axis=0)
        added = jnp.dot(both, returned[c].reshape(chunk_slots, width), preferred_element_type=f32)
        result = result + (added[:tok_rows] + added[tok_rows:])
    return result.astype(bf16)


def solution(mesh):
    placed = (
        P(("sp", "tp"), None),
        P("sp", "tp"),
        P("sp", "tp"),
        P("sp", "tp"),
        P("sp"),
        P(None, "tp"),
        P(),
        P(),
        P(("sp", "tp"), None),
        P(("sp", "tp"), None),
        P(("sp", "tp")),
        P(("sp", "tp"), None, None),
        P(("sp", "tp"), None, None),
        P(("sp", "tp"), None, None),
    )
    return jax.shard_map(
        on_device, mesh=mesh, in_specs=placed, out_specs=P(("sp", "tp"), None), check_vma=False
    )
```

time: 170 us -> 149 us (0.88)
  local copies, waits for them, and re-layouts: 14.3 us -> 5.6 us
  other arithmetic: 12.6 us -> 4.92 us
  starting transfers between devices: 16.3 us -> 9.83 us
    ppermute x4 -> x2, starting transfers between devices: 12.5 us -> 6.16 us  [the longest x1 4.87 us: on_device(): before = lax.ppermute(edge(slice(-1, None)), 'sp', up)]
    gather x2 -> x0, local copies, waits for them, and re-layouts: 5.69 us -> none  [the longest x1 3.35 us: on_device(): normed[source_row]]
    reduce_sum x2 -> x0, other arithmetic: 3.26 us -> none  [the longest x1 3.16 us: on_device(): result = resid + jnp.sum(gate[:, :, None] * picked, axis=1)]
    scatter x2 -> x0, local copies, waits for them, and re-layouts: 2.88 us -> none  [the longest x1 1.49 us: on_device(): filled = jnp.zeros((slot_count,), jnp.bool_).at[slot].set(True)]
    convert_element_type x1 -> x0, local copies, waits for them, and re-layouts: 2.37 us -> none  [on_device(): picked = returned.reshape(slot_count, width)[slot].astype(jnp.float32).re...]
    select_n x4 -> x0, other arithmetic: 1.81 us -> none  [the longest x1 1.8 us: on_device(): jnp.where(filled[:, None], normed[source_row], jnp.zeros((), jnp.bfloat16))]
    slice x4 -> x8, local copies, waits for them, and re-layouts: 1.6 us -> 3.39 us  [the longest x1 0.83 us: on_device(): docs_prev = jnp.concatenate([doc_before, doc_ids[:-1]])]
    dot_general x3 -> x7, matrix products: 16.6 us -> 17.9 us  [the longest x1 9.93 us: on_device(): jnp.dot(hidden, w_down[0], preferred_element_type=f32).astype(bf16)]
  transfers between devices with their start and end apart: 5 -> 3, of which waited for: 1 -> 1; matrix products, arithmetic and copies ran while one was open for 6% -> 3% of each run, Pallas kernels for 0% -> 0%
where the time goes in v1:
time: 149 us; the launch traced here: 148 us
  blocking collectives  59.7 us (40%)
  waiting for transfers between devices  48.5 us (33%)
  matrix products  17.9 us (12%)
  starting transfers between devices  9.83 us (7%)
  local copies, waits for them, and re-layouts  5.6 us (4%)
  other arithmetic  4.92 us (3%)
  between operations  1.52 us (1%)
    all_to_all x1, blocking collectives, on_device(): lax.all_to_all(outgoing.reshape(expert_total, part, width), ('sp', 'tp'),...  55.5 us
    all_to_all x1, waiting for transfers between devices, on_device(): lax.all_to_all(outputs.reshape(expert_total, part, width), ('sp', 'tp'),...  48.5 us
    dot_general x1, matrix products, on_device(): jnp.dot(hidden, w_down[0], preferred_element_type=f32).astype(bf16)  9.93 us
    ppermute x1, starting transfers between devices, on_device(): before = lax.ppermute(edge(slice(-1, None)), 'sp', up)  4.87 us
    all_to_all x1, blocking collectives, on_device(): lax.all_to_all(mixed.reshape(-1, tok_rows, channels_here), 'tp', split_ax...  4.21 us
    dot_general x1, matrix products, on_device(): jnp.dot(rows_in, w_gate[0], preferred_element_type=f32)  3.72 us
    all_to_all x1, starting transfers between devices, on_device(): lax.all_to_all(outputs.reshape(expert_total, part, width), ('sp', 'tp'),...  3.67 us
  transfers between devices with their start and end apart: 3, of which 1 were waited for; matrix products, arithmetic and copies ran while one was open for 3% of the time, Pallas kernels for 0%

profile of v1, /device:TPU:0, one launch (start us, length us, event | category | flops | bytes accessed | tf_op | source)
XLA Modules:
  0.0 148.0 jit_solution(1177211332271703396)
XLA Ops:
  0.0 0.0 copy-start.2
  0.0 0.0 copy-start.1
  0.0 0.8 convert.6
  0.8 0.6 fusion.46
  1.4 0.8 multiply_convert_fusion.5
  2.2 0.6 concatenate.21
  2.8 4.9 %collective-permute-start = (bf16[1,640]{1,0:T(2,128)(2,1)S(1)}, bf16[1,640]{1,0:T(2,128)(2,1)S(1)}, u32[]{:S(2)}, u32[]{:S(2)}) collective-permute-start(bf16[1,640]{1,0:T(2,128)(2,1)S(1)} %concatenate.21), channel_id=1, source_target_pairs={{0,2},{2,4},{4,6},{6,8},{8,10},{10,12},{12,14},{14,16},{16,18},{18... | collective-permute-start | bytes 3848 | tf_op jit(solution)/shard_map/ppermute | solution.py:41
  7.7 0.7 concatenate.24
  8.3 1.3 collective-permute-start.1
  9.6 0.8 fusion.45
  10.5 1.1 multiply_convert_fusion.4
  11.6 0.1 fusion.43
  11.6 0.8 fusion.44
  12.5 0.8 slice_bitcast_fusion.11
  13.2 0.2 select_reduce_fusion.1
  13.4 0.0 collective-permute-done
  13.4 0.5 slice.126
  14.6 0.0 collective-permute-done.1
  14.6 0.5 slice.129
  15.8 0.8 compare_convert_fusion.1
  16.6 0.0 copy-done.2
  16.6 0.3 multiply_convert_fusion.3
  16.9 0.0 copy-start
  16.9 4.2 %all_to_all.15 = bf16[2,128,512]{2,1,0:T(8,128)(2,1)S(1)} all-to-all(bf16[2,128,512]{2,1,0:T(8,128)(2,1)S(1)} %bitcast.63), channel_id=1, replica_groups=mesh['sp'=16,'tp'=2] {'tp'}, dimensions={0} | all-to-all | bytes 524288 | tf_op jit(solution)/shard_map/all_to_all | solution.py:77
  21.1 0.0 copy-done.1
  21.1 2.1 %convolution_add_fusion.1 = f32[128,2048]{1,0:T(8,128)S(1)} fusion(bf16[1024,2048]{1,0:T(8,128)(2,1)} %param.20, bf16[128,2048]{1,0:T(8,128)(2,1)S(1)} %copy-done.1, bf16[2,128,512]{2,1,0:T(8,128)(2,1)S(1)} %all_to_all.15), kind=kOutput, calls=%fused_computation.9 | convolution fusion | flops 268959744 | bytes 3801088 | tf_op jit(solution)/shard_map/dot_general | solution.py:83
  23.2 0.0 copy-done
  23.2 0.0 copy-start.3
  23.2 0.5 multiply_reduce_fusion
  23.7 0.1 copy-done.3
  23.9 0.8 convolution_convert_fusion
  24.7 0.0 copy-start.6
  24.7 55.5 %all_to_all.16 = bf16[32,16,2048]{2,1,0:T(8,128)(2,1)S(1)} all-to-all(bf16[32,16,2048]{2,1,0:T(8,128)(2,1)S(1)} %bitcast.59), channel_id=1, replica_groups=mesh['sp'=16,'tp'=2] {'sp','tp'}, dimensions={0} | all-to-all | bytes 4194304 | tf_op jit(solution)/shard_map/all_to_all | solution.py:95
  80.2 0.0 copy-done.6
  80.2 3.7 %fusion.4 = f32[512,1024]{1,0:T(8,128)} fusion(bf16[512,2048]{1,0:T(8,128)(2,1)S(1)} %bitcast.61, bf16[1,2048,1024]{2,1,0:T(8,128)(2,1)S(1)} %copy-done.6), kind=kOutput, calls=%fused_computation.4 | convolution fusion | flops 2147483648 | bytes 8388608 | tf_op jit(solution)/shard_map/dot_general | solution.py:104
  83.9 9.9 %fusion.6 = bf16[512,2048]{1,0:T(8,128)(2,1)} fusion(bf16[1,1024,2048]{2,1,0:T(8,128)(2,1)} %param.27, f32[512,1024]{1,0:T(8,128)} %fusion.4, bf16[512,2048]{1,0:T(8,128)(2,1)S(1)} %bitcast.62, bf16[1,2048,1024]{2,1,0:T(8,128)(2,1)} %param.26), kind=kOutput, calls=%fused_computation.6 | convolution fusion | flops 4299161600 | bytes 14680064 | tf_op jit(solution)/shard_map/dot_general | solution.py:107
  93.8 0.0 copy-start.4
  93.8 0.0 copy-start.5
  93.8 3.7 %all-to-all-start.2 = ((bf16[32,16,2048]{2,1,0:T(8,128)(2,1)}), bf16[32,16,2048]{2,1,0:T(8,128)(2,1)S(1)}, u32[]{:S(2)}, u32[]{:S(2)}) async-start(bf16[32,16,2048]{2,1,0:T(8,128)(2,1)} %bitcast.60), calls=%async_computation.2 | async-start | bytes 4194304 | tf_op jit(solution)/shard_map/all_to_all | solution.py:109
  97.5 0.0 copy-done.4
  97.5 0.0 copy-done.5
  97.5 0.2 reduce-precision_convert_fusion
  97.7 48.5 %all-to-all-done.2 = bf16[32,16,2048]{2,1,0:T(8,128)(2,1)S(1)} async-done(((bf16[32,16,2048]{2,1,0:T(8,128)(2,1)}), bf16[32,16,2048]{2,1,0:T(8,128)(2,1)S(1)}, u32[]{:S(2)}, u32[]{:S(2)}) %all-to-all-start.2) | async-done | bytes 2097184 | tf_op jit(solution)/shard_map/all_to_all | solution.py:109
  146.2 0.7 fusion.20
  146.9 1.0 fusion.14
  (8 shorter events, 0.1 us)
Async XLA Ops:
  0.0 16.6 %copy-start.2 = (bf16[256,512]{1,0:T(8,128)(2,1)S(1)}, bf16[256,512]{1,0:T(8,128)(2,1)}, u32[]{:S(2)}) copy-start(bf16[256,512]{1,0:T(8,128)(2,1)} %param.15) | copy-start | bytes 786436
  0.0 21.1 %copy-start.1 = (bf16[128,2048]{1,0:T(8,128)(2,1)S(1)}, bf16[128,2048]{1,0:T(8,128)(2,1)}, u32[]{:S(2)}) copy-start(bf16[128,2048]{1,0:T(8,128)(2,1)} %param.14) | copy-start | bytes 1572868
  2.8 10.6 %collective-permute-start = (bf16[1,640]{1,0:T(2,128)(2,1)S(1)}, bf16[1,640]{1,0:T(2,128)(2,1)S(1)}, u32[]{:S(2)}, u32[]{:S(2)}) collective-permute-start(bf16[1,640]{1,0:T(2,128)(2,1)S(1)} %concatenate.21), channel_id=1, source_target_pairs={{0,2},{2,4},{4,6},{6,8},{8,10},{10,12},{12,14},{14,16},{16,18},{18... | collective-permute-start | bytes 3848 | tf_op jit(solution)/shard_map/ppermute | solution.py:41
  8.3 6.3 %collective-permute-start.1 = (bf16[1,640]{1,0:T(2,128)(2,1)S(1)}, bf16[1,640]{1,0:T(2,128)(2,1)S(1)}, u32[]{:S(2)}, u32[]{:S(2)}) collective-permute-start(bf16[1,640]{1,0:T(2,128)(2,1)S(1)} %concatenate.24), channel_id=1, source_target_pairs={{2,0},{4,2},{6,4},{8,6},{10,8},{12,10},{14,12},{16,14},{18,16},{20... | collective-permute-start | bytes 3848 | tf_op jit(solution)/shard_map/ppermute | solution.py:42
  16.9 6.3 %copy-start = (bf16[1024,2048]{1,0:T(8,128)(2,1)S(1)}, bf16[1024,2048]{1,0:T(8,128)(2,1)}, u32[]{:S(2)}) copy-start(bf16[1024,2048]{1,0:T(8,128)(2,1)} %param.20) | copy-start | bytes 12582916
  23.2 0.7 copy-start.3
  24.7 55.5 %copy-start.6 = (bf16[1,2048,1024]{2,1,0:T(8,128)(2,1)S(1)}, bf16[1,2048,1024]{2,1,0:T(8,128)(2,1)}, u32[]{:S(2)}) copy-start(bf16[1,2048,1024]{2,1,0:T(8,128)(2,1)} %param.25) | copy-start | bytes 12582916
  93.8 3.7 %copy-start.4 = (f32[128,2]{0,1:T(2,128)S(1)}, f32[128,2]{0,1:T(2,128)}, u32[]{:S(2)}) copy-start(f32[128,2]{0,1:T(2,128)} %param.23) | copy-start | bytes 3076
  93.8 3.7 %copy-start.5 = (f32[128]{0:T(128)S(1)}, f32[128]{0:T(128)}, u32[]{:S(2)}) copy-start(f32[128]{0:T(128)} %param.24) | copy-start | bytes 1540
  93.8 52.4 %all-to-all-start.2 = ((bf16[32,16,2048]{2,1,0:T(8,128)(2,1)}), bf16[32,16,2048]{2,1,0:T(8,128)(2,1)S(1)}, u32[]{:S(2)}, u32[]{:S(2)}) async-start(bf16[32,16,2048]{2,1,0:T(8,128)(2,1)} %bitcast.60), calls=%async_computation.2 | async-start | bytes 4194304 | tf_op jit(solution)/shard_map/all_to_all | solution.py:109

commit v2 on v1

--- a/solution.py
+++ b/solution.py
@@ -1,9 +1,107 @@
 import jax
 import jax.numpy as jnp
 from jax import lax
+from jax.experimental import pallas as pl
+from jax.experimental.pallas import tpu as pltpu
 from jax.sharding import PartitionSpec as P
 
 CHUNKS = 1
+LANES = 128
+
+
+def edge_rows(inner_gate, conv_values, doc_ids):
+    rows, chans = inner_gate.shape
+    tile = 16
+    last = rows // tile - 1
+
+    def body(doc, in_first, in_last, val_first, val_last, first, final):
+        for out, a, b, at, row in (
+            (first, in_first, val_first, 0, 0),
+            (final, in_last, val_last, rows - 1, tile - 1),
+        ):
+            product = a[...].astype(jnp.float32) * b[...].astype(jnp.float32)
+            out[:, :chans] = product[row : row + 1].astype(jnp.bfloat16)
+            number = doc[at].astype(jnp.float32)
+            out[:, chans:] = jnp.full((1, LANES), number, jnp.float32).astype(jnp.bfloat16)
+
+    head = pl.BlockSpec((tile, chans), lambda i: (0, 0))
+    tail = pl.BlockSpec((tile, chans), lambda i: (last, 0))
+    whole = pl.BlockSpec((1, chans + LANES), lambda i: (0, 0))
+    row = jax.ShapeDtypeStruct((1, chans + LANES), jnp.bfloat16)
+    return pl.pallas_call(
+        body,
+        grid=(1,),
+        in_specs=[pl.BlockSpec(memory_space=pltpu.SMEM), head, tail, head, tail],
+        out_specs=[whole, whole],
+        out_shape=[row, row],
+    )(doc_ids, inner_gate, inner_gate, conv_values, conv_values)
+
+
+def masked_conv(inner_gate, conv_values, outer_gate, doc_ids, conv_taps, before, after):
+    rows, chans = inner_gate.shape
+    f32 = jnp.float32
+
+    def body(inner, values, outer, docs, taps, prev_edge, next_edge, out):
+        product = (inner[...].astype(f32) * values[...].astype(f32)).astype(jnp.bfloat16)
+        product = product.astype(f32)
+        row_at = lax.broadcasted_iota(jnp.int32, (rows, rows), 0)
+        col_at = lax.broadcasted_iota(jnp.int32, (rows, rows), 1)
+        doc_row = docs[...].astype(f32)
+
+        def column(offset):
+            kept = jnp.where(col_at == row_at + offset, doc_row, 0.0)
+            return jnp.sum(kept, axis=1, keepdims=True)
+
+        at = lax.broadcasted_iota(jnp.int32, (rows, 1), 0)
+        own = column(0)
+        prev_doc = jnp.where(at == 0, prev_edge[:, chans : chans + 1].astype(f32), column(-1))
+        next_doc = jnp.where(at == rows - 1, next_edge[:, chans : chans + 1].astype(f32), column(1))
+        same_prev = (prev_doc == own).astype(f32)
+        same_next = (next_doc == own).astype(f32)
+        prod_prev = jnp.where(at == 0, prev_edge[:, :chans].astype(f32), pltpu.roll(product, 1, 0))
+        prod_next = jnp.where(
+            at == rows - 1, next_edge[:, :chans].astype(f32), pltpu.roll(product, rows - 1, 0)
+        )
+        conv = (
+            taps[0:1] * prod_prev * same_prev
+            + taps[1:2] * product
+            + taps[2:3] * prod_next * same_next
+        )
+        out[...] = (outer[...].astype(f32) * conv).astype(jnp.bfloat16)
+
+    return pl.pallas_call(
+        body, out_shape=jax.ShapeDtypeStruct((rows, chans), jnp.bfloat16)
+    )(inner_gate, conv_values, outer_gate, doc_ids.reshape(1, rows), conv_taps, before, after)
+
+
+def expert_mlp(rows_in, w_gate, w_up, w_down):
+    count, width = rows_in.shape
+    inner = w_gate.shape[1]
+    first, second = 4, 4
+    f_block, d_block = inner // first, width // second
+    f32 = jnp.float32
+
+    def body(x, gate, up, down, out, hidden):
+        for f in range(first):
+            here = slice(f * f_block, (f + 1) * f_block)
+            g = jnp.dot(x[...], gate[:, here], preferred_element_type=f32)
+            u = jnp.dot(x[...], up[:, here], preferred_element_type=f32)
+            hidden[:, here] = (g / (1.0 + jnp.exp(-g)) * u).astype(jnp.bfloat16)
+        for d in range(second):
+            here = slice(d * d_block, (d + 1) * d_block)
+            out[:, here] = jnp.dot(
+                hidden[...], down[:, here], preferred_element_type=f32
+            ).astype(out.dtype)
+
+    vmem = pl.BlockSpec(memory_space=pltpu.VMEM)
+    return pl.pallas_call(
+        body,
+        in_specs=[vmem, vmem, vmem, vmem],
+        out_specs=vmem,
+        out_shape=jax.ShapeDtypeStruct((count, width), jnp.bfloat16),
+        scratch_shapes=[pltpu.VMEM((count, inner), jnp.bfloat16)],
+        compiler_params=pltpu.CompilerParams(vmem_limit_bytes=32 << 20),
+    )(rows_in, w_gate, w_up, w_down)
 
 
 def on_device(
@@ -26,20 +124,12 @@
     tok_rows, width = stream.shape
     channels_here = inner_gate.shape[1]
 
-    def gated(rows):
-        return (inner_gate[rows].astype(f32) * conv_values[rows].astype(f32)).astype(bf16)
-
     sp = lax.axis_size("sp")
     up = [(i, (i + 1) % sp) for i in range(sp - 1)]
     down = [(j, i) for i, j in up]
-    lanes = 128
-
-    def edge(rows):
-        doc = jnp.broadcast_to(doc_ids[rows].astype(bf16)[:, None], (1, lanes))
-        return jnp.concatenate([gated(rows), doc], axis=1)
-
-    before = lax.ppermute(edge(slice(-1, None)), "sp", up)
-    after = lax.ppermute(edge(slice(0, 1)), "sp", down)
+    leading, last = edge_rows(inner_gate, conv_values, doc_ids)
+    before = lax.ppermute(last, "sp", up)
+    after = lax.ppermute(leading, "sp", down)
 
     expert_total = lax.axis_size("sp") * lax.axis_size("tp")
     top_count = route_ids.shape[1]
@@ -58,22 +148,9 @@
     expo = jnp.exp(route_logits)
     gate = group_weight[:, None] * expo / jnp.sum(expo, axis=1, keepdims=True)
 
-    product = gated(slice(None))
-    prod = product.astype(f32)
-    doc_before = before[:, channels_here].astype(jnp.int32)
-    doc_after = after[:, channels_here].astype(jnp.int32)
-    docs_prev = jnp.concatenate([doc_before, doc_ids[:-1]])
-    docs_next = jnp.concatenate([doc_ids[1:], doc_after])
-    same_prev = (docs_prev == doc_ids).astype(f32)[:, None]
-    same_next = (docs_next == doc_ids).astype(f32)[:, None]
-    prod_prev = jnp.concatenate([before[:, :channels_here], product[:-1]], axis=0).astype(f32)
-    prod_next = jnp.concatenate([product[1:], after[:, :channels_here]], axis=0).astype(f32)
-    conv = (
-        conv_taps[0] * prod_prev * same_prev
-        + conv_taps[1] * prod
-        + conv_taps[2] * prod_next * same_next
-    )
-    mixed = (outer_gate.astype(f32) * conv).astype(bf16)
+    mixed = masked_conv(
+        inner_gate, conv_values, outer_gate, doc_ids, conv_taps, before, after
+    )
     halves = lax.all_to_all(
         mixed.reshape(-1, tok_rows, channels_here), "tp", split_axis=0, concat_axis=0, tiled=True
     )
@@ -100,11 +177,7 @@
     returned = []
     for c in range(CHUNKS):
         rows_in = arrived[c].reshape(chunk_slots, width)
-        hidden = (
-            jax.nn.silu(jnp.dot(rows_in, w_gate[0], preferred_element_type=f32))
-            * jnp.dot(rows_in, w_up[0], preferred_element_type=f32)
-        ).astype(bf16)
-        outputs = jnp.dot(hidden, w_down[0], preferred_element_type=f32).astype(bf16)
+        outputs = expert_mlp(rows_in, w_gate[0], w_up[0], w_down[0])
         returned.append(
             lax.all_to_all(
                 outputs.reshape(expert_total, part, width),

time: 149 us -> 143 us (0.960)
  Pallas kernels: 0 us -> 11.8 us
  matrix products: 17.9 us -> 6.18 us
  local copies, waits for them, and re-layouts: 5.6 us -> 1.36 us
  other arithmetic: 4.92 us -> 1.25 us
  waiting for transfers between devices: 48.5 us -> 51.9 us
    dot_general x2 -> x0, matrix products: 13.6 us -> none  [the longest x1 9.93 us: on_device(): jnp.dot(hidden, w_down[0], preferred_element_type=f32).astype(bf16)]
    pallas_call x0 -> x3, Pallas kernels: none -> 11.8 us  [the longest x1 8.04 us: expert_mlp(): pl.pallas_call(body, in_specs=[vmem, vmem, vmem, vmem], out_specs=vmem, o...]
    ppermute x2, waiting for transfers between devices: 0.01 us -> 3.41 us  [the longest x1 3.4 us: on_device(): after = lax.ppermute(leading, 'sp', down)]
    slice x8 -> x0, local copies, waits for them, and re-layouts: 3.39 us -> none  [the longest x1 0.83 us: on_device(): docs_prev = jnp.concatenate([doc_before, doc_ids[:-1]])]
    convert_element_type x4 -> x0, other arithmetic: 2.91 us -> none  [the longest x2 1.85 us: gated(): (inner_gate[rows].astype(f32) * conv_values[rows].astype(f32)).astype(bf16)]
    dot_general x2, matrix products: 2.6 us -> 4.53 us  [on_device(): resid = resid + jnp.dot(halves[i], weights[i], preferred_element_type=f32)]
  transfers between devices with their start and end apart: 3 -> 3, of which waited for: 1 -> 2; matrix products, arithmetic and copies ran while one was open for 3% -> 1% of each run, Pallas kernels for 0% -> 0%
where the time goes in v2:
time: 143 us
  blocking collectives  60.1 us (42%)
  waiting for transfers between devices  51.9 us (36%)
  Pallas kernels  11.8 us (8%)
  starting transfers between devices  9.81 us (7%)
  matrix products  6.18 us (4%)
    all_to_all x1, blocking collectives, on_device(): lax.all_to_all(outgoing.reshape(expert_total, part, width), ('sp', 'tp'),...  55.1 us
    all_to_all x1, waiting for transfers between devices, on_device(): lax.all_to_all(outputs.reshape(expert_total, part, width), ('sp', 'tp'),...  48.5 us
    pallas_call x1, Pallas kernels, expert_mlp(): pl.pallas_call(body, in_specs=[vmem, vmem, vmem, vmem], out_specs=vmem, o...  8.04 us
    all_to_all x1, blocking collectives, on_device(): lax.all_to_all(mixed.reshape(-1, tok_rows, channels_here), 'tp', split_ax...  4.98 us
    ppermute x1, starting transfers between devices, on_device(): before = lax.ppermute(last, 'sp', up)  4.86 us
    dot_general x2, matrix products, on_device(): resid = resid + jnp.dot(halves[i], weights[i], preferred_element_type=f32)  4.53 us
    all_to_all x1, starting transfers between devices, on_device(): lax.all_to_all(outputs.reshape(expert_total, part, width), ('sp', 'tp'),...  3.66 us
    ppermute x1, waiting for transfers between devices, on_device(): after = lax.ppermute(leading, 'sp', down)  3.4 us
  transfers between devices with their start and end apart: 3, of which 2 were waited for; matrix products, arithmetic and copies ran while one was open for 1% of the time, Pallas kernels for 0%

profile of v2, /device:TPU:0, one launch (start us, length us, event | category | flops | bytes accessed | tf_op | source)
XLA Modules:
  0.0 142.6 jit_solution(6139518420702533034)
XLA Ops:
  0.0 0.0 copy-start.3
  0.0 1.4 %shard_map.136 = (bf16[1,640]{1,0:T(2,128)(2,1)}, bf16[1,640]{1,0:T(2,128)(2,1)}) custom-call(s32[256]{0:T(256)} %doc.1, bf16[256,512]{1,0:T(8,128)(2,1)} %inner.1, bf16[256,512]{1,0:T(8,128)(2,1)} %inner.1, bf16[256,512]{1,0:T(8,128)(2,1)} %values.1, bf16[256,512]{1,0:T(8,128)(2,1)} %values.1), custom_call_target="tpu_custom_call" | custom-call | tf_op jit(solution)/shard_map/pallas_call | solution.py:31
  1.4 4.9 %collective-permute-start = (bf16[1,640]{1,0:T(2,128)(2,1)}, bf16[1,640]{1,0:T(2,128)(2,1)S(1)}, u32[]{:S(2)}, u32[]{:S(2)}) collective-permute-start(bf16[1,640]{1,0:T(2,128)(2,1)} %get-tuple-element.7), channel_id=1, source_target_pairs={{0,2},{2,4},{4,6},{6,8},{8,10},{10,12},{12,14},{14,16},{16,18},{18... | collective-permute-start | bytes 3848 | tf_op jit(solution)/shard_map/ppermute | solution.py:131
  6.3 1.3 collective-permute-start.1
  7.6 0.8 slice_bitcast_fusion.11
  8.4 0.2 select_reduce_fusion.1
  8.6 0.0 collective-permute-done.prev_edge
  8.6 0.0 copy-start.5
  8.6 3.4 %collective-permute-done.1.next_edge = bf16[1,640]{1,0:T(2,128)(2,1)S(1)} collective-permute-done((bf16[1,640]{1,0:T(2,128)(2,1)}, bf16[1,640]{1,0:T(2,128)(2,1)S(1)}, u32[]{:S(2)}, u32[]{:S(2)}) %collective-permute-start.1) | collective-permute-done | bytes 1312 | tf_op jit(solution)/shard_map/ppermute | solution.py:132
  12.0 0.0 copy-start.6
  12.0 0.0 copy-done.5
  12.0 0.6 copy-done.6
  12.6 2.3 %shard_map.137 = bf16[256,512]{1,0:T(8,128)(2,1)} custom-call(bf16[256,512]{1,0:T(8,128)(2,1)} %inner.1, bf16[256,512]{1,0:T(8,128)(2,1)} %values.1, bf16[256,512]{1,0:T(8,128)(2,1)} %outer.1, s32[1,256]{1,0:T(1,128)} %bitcast.43, f32[3,512]{1,0:T(4,128)} %taps.1, bf16[1,640]{1,0:T(2,128)(2,1)} %copy-done.5, bf16[1,640]{1,0:T(2,128)(2,1)} %copy-done.6), custom_call_target="tpu_custom_call" | custom-call | tf_op jit(solution)/shard_map/pallas_call | solution.py:72
  14.9 5.0 %all_to_all.15 = bf16[2,128,512]{2,1,0:T(8,128)(2,1)S(1)} all-to-all(bf16[2,128,512]{2,1,0:T(8,128)(2,1)} %bitcast.42), channel_id=1, replica_groups=mesh['sp'=16,'tp'=2] {'tp'}, dimensions={0} | all-to-all | bytes 524288 | tf_op jit(solution)/shard_map/all_to_all | solution.py:154
  19.9 0.0 copy-done.3
  19.9 0.0 copy-start.4
  19.9 0.0 copy-start.2
  19.9 2.2 %convolution_add_fusion.1 = f32[128,2048]{1,0:T(8,128)S(1)} fusion(bf16[1024,2048]{1,0:T(8,128)(2,1)} %param.20, bf16[128,2048]{1,0:T(8,128)(2,1)S(1)} %copy-done.3, bf16[2,128,512]{2,1,0:T(8,128)(2,1)S(1)} %all_to_all.15), kind=kOutput, calls=%fused_computation.2 | convolution fusion | flops 268959744 | bytes 3801088 | tf_op jit(solution)/shard_map/dot_general | solution.py:160
  22.1 0.0 copy-start.1
  22.1 2.3 %multiply_reduce_fusion = (f32[128]{0:T(128)S(1)}, f32[128,2048]{1,0:T(8,128)S(1)}) fusion(f32[128,2048]{1,0:T(8,128)S(1)} %convolution_add_fusion.1, bf16[1024,2048]{1,0:T(8,128)(2,1)} %param.20, bf16[2,128,512]{2,1,0:T(8,128)(2,1)S(1)} %all_to_all.15), kind=kOutput, calls=%fused_computation.9 | convolution fusion | flops 269221760 | bytes 4325888 | tf_op jit(solution)/shard_map/dot_general | solution.py:160
  24.5 0.0 copy-done.4
  24.5 0.8 convolution_convert_fusion
  25.3 0.0 copy-start
  25.3 55.1 %all_to_all.16 = bf16[32,16,2048]{2,1,0:T(8,128)(2,1)S(1)} all-to-all(bf16[32,16,2048]{2,1,0:T(8,128)(2,1)S(1)} %bitcast.41), channel_id=1, replica_groups=mesh['sp'=16,'tp'=2] {'sp','tp'}, dimensions={0} | all-to-all | bytes 4194304 | tf_op jit(solution)/shard_map/all_to_all | solution.py:172
  80.4 0.0 copy-done.2
  80.4 0.0 copy-done.1
  80.4 0.0 copy-done
  80.4 8.0 %shard_map.138 = bf16[512,2048]{1,0:T(8,128)(2,1)} custom-call(bf16[512,2048]{1,0:T(8,128)(2,1)S(1)} %bitcast.36, bf16[2048,1024]{1,0:T(8,128)(2,1)S(1)} %bitcast.37, bf16[2048,1024]{1,0:T(8,128)(2,1)S(1)} %bitcast.38, bf16[1024,2048]{1,0:T(8,128)(2,1)S(1)} %bitcast.39), custom_call_target="tpu_custom_call" | custom-call | tf_op jit(solution)/shard_map/pallas_call | solution.py:97
  88.4 0.0 copy-start.7
  88.4 0.0 copy-start.8
  88.4 3.7 %all-to-all-start.2 = ((bf16[32,16,2048]{2,1,0:T(8,128)(2,1)}), bf16[32,16,2048]{2,1,0:T(8,128)(2,1)S(1)}, u32[]{:S(2)}, u32[]{:S(2)}) async-start(bf16[32,16,2048]{2,1,0:T(8,128)(2,1)} %bitcast.19), calls=%async_computation.2 | async-start | bytes 4194304 | tf_op jit(solution)/shard_map/all_to_all | solution.py:182
  92.1 0.0 copy-done.7
  92.1 0.0 copy-done.8
  92.2 0.2 reduce-precision_convert_fusion
  92.3 48.5 %all-to-all-done.2 = bf16[32,16,2048]{2,1,0:T(8,128)(2,1)S(1)} async-done(((bf16[32,16,2048]{2,1,0:T(8,128)(2,1)}), bf16[32,16,2048]{2,1,0:T(8,128)(2,1)S(1)}, u32[]{:S(2)}, u32[]{:S(2)}) %all-to-all-start.2) | async-done | bytes 2097184 | tf_op jit(solution)/shard_map/all_to_all | solution.py:182
  140.8 0.7 fusion.7
  141.6 1.0 fusion.3
  (6 shorter events, 0.1 us)
Async XLA Ops:
  0.0 19.9 %copy-start.3 = (bf16[128,2048]{1,0:T(8,128)(2,1)S(1)}, bf16[128,2048]{1,0:T(8,128)(2,1)}, u32[]{:S(2)}) copy-start(bf16[128,2048]{1,0:T(8,128)(2,1)} %param.14) | copy-start | bytes 1572868
  1.4 7.1 %collective-permute-start = (bf16[1,640]{1,0:T(2,128)(2,1)}, bf16[1,640]{1,0:T(2,128)(2,1)S(1)}, u32[]{:S(2)}, u32[]{:S(2)}) collective-permute-start(bf16[1,640]{1,0:T(2,128)(2,1)} %get-tuple-element.7), channel_id=1, source_target_pairs={{0,2},{2,4},{4,6},{6,8},{8,10},{10,12},{12,14},{14,16},{16,18},{18... | collective-permute-start | bytes 3848 | tf_op jit(solution)/shard_map/ppermute | solution.py:131
  6.3 5.7 %collective-permute-start.1 = (bf16[1,640]{1,0:T(2,128)(2,1)}, bf16[1,640]{1,0:T(2,128)(2,1)S(1)}, u32[]{:S(2)}, u32[]{:S(2)}) collective-permute-start(bf16[1,640]{1,0:T(2,128)(2,1)} %get-tuple-element.8), channel_id=1, source_target_pairs={{2,0},{4,2},{6,4},{8,6},{10,8},{12,10},{14,12},{16,14},{18,16},{20... | collective-permute-start | bytes 3848 | tf_op jit(solution)/shard_map/ppermute | solution.py:132
  8.6 3.4 %copy-start.5 = (bf16[1,640]{1,0:T(2,128)(2,1)}, bf16[1,640]{1,0:T(2,128)(2,1)S(1)}, u32[]{:S(2)}) copy-start(bf16[1,640]{1,0:T(2,128)(2,1)S(1)} %collective-permute-done.prev_edge) | copy-start | bytes 3844
  12.0 0.6 copy-start.6
  19.9 4.6 %copy-start.4 = (f32[2048]{0:T(1024)S(1)}, f32[2048]{0:T(1024)}, u32[]{:S(2)}) copy-start(f32[2048]{0:T(1024)} %param.21) | copy-start | bytes 24580
  19.9 60.5 %copy-start.2 = (bf16[1,1024,2048]{2,1,0:T(8,128)(2,1)S(1)}, bf16[1,1024,2048]{2,1,0:T(8,128)(2,1)}, u32[]{:S(2)}) copy-start(bf16[1,1024,2048]{2,1,0:T(8,128)(2,1)} %param.27) | copy-start | bytes 12582916
  22.1 58.3 %copy-start.1 = (bf16[1,2048,1024]{2,1,0:T(8,128)(2,1)S(1)}, bf16[1,2048,1024]{2,1,0:T(8,128)(2,1)}, u32[]{:S(2)}) copy-start(bf16[1,2048,1024]{2,1,0:T(8,128)(2,1)} %param.26) | copy-start | bytes 12582916
  25.3 55.1 %copy-start = (bf16[1,2048,1024]{2,1,0:T(8,128)(2,1)S(1)}, bf16[1,2048,1024]{2,1,0:T(8,128)(2,1)}, u32[]{:S(2)}) copy-start(bf16[1,2048,1024]{2,1,0:T(8,128)(2,1)} %param.25) | copy-start | bytes 12582916
  88.4 3.7 %copy-start.7 = (f32[128,2]{0,1:T(2,128)S(1)}, f32[128,2]{0,1:T(2,128)}, u32[]{:S(2)}) copy-start(f32[128,2]{0,1:T(2,128)} %param.23) | copy-start | bytes 3076
  88.4 3.7 %copy-start.8 = (f32[128]{0:T(128)S(1)}, f32[128]{0:T(128)}, u32[]{:S(2)}) copy-start(f32[128]{0:T(128)} %param.24) | copy-start | bytes 1540
  88.4 52.4 %all-to-all-start.2 = ((bf16[32,16,2048]{2,1,0:T(8,128)(2,1)}), bf16[32,16,2048]{2,1,0:T(8,128)(2,1)S(1)}, u32[]{:S(2)}, u32[]{:S(2)}) async-start(bf16[32,16,2048]{2,1,0:T(8,128)(2,1)} %bitcast.19), calls=%async_computation.2 | async-start | bytes 4194304 | tf_op jit(solution)/shard_map/all_to_all | solution.py:182
